TPU v7x, 32 devices: a whole 2x2x4 slice. The times are simulated.
32 devices in a mesh: ep: 4 (over y, x), tp: 8 (over z, core).
Axes of the slice: x: 2, y: 2, z: 4, core: 2. Of those that a mesh axis runs over, the one named last changes fastest.
Arguments:
- pool_input: bfloat16 [4096, 1024], P('ep', 'tp'), may hold values from -6 to 6
- pool_gain: float32 [1024], P('tp'), may hold values from 0.1 to 1.9
- mix_weight: bfloat16 [1024, 2048], P('tp'), may hold values from -0.1875 to 0.1875
- moe_input: bfloat16 [8192, 2048], P(('ep', 'tp')), may hold values from -6 to 6
- moe_gain: float32 [2048], replicated, may hold values from 0.1 to 1.9
- expert_ids: int32 [8192, 2], P(('ep', 'tp')), may hold values from 0 to 15, as said below
- route_weight: float32 [8192, 2], P(('ep', 'tp')), may hold values from 0.2 to 1
- gate_weight: bfloat16 [16, 2048, 1024], P('ep', None, 'tp'), may hold values from -0.125 to 0.125
- up_weight: bfloat16 [16, 2048, 1024], P('ep', None, 'tp'), may hold values from -0.125 to 0.125
- down_weight: bfloat16 [16, 2048, 1024], P('ep', None, 'tp'), may hold values from -0.1875 to 0.1875
Outputs:
- mixed_out: bfloat16 [4096, 2048], P(('ep', 'tp'))
- moe_out: bfloat16 [8192, 2048], P(('ep', 'tp'))
Inputs may be any that keep to these rules, and one draw needn't show every extreme that they name: `expert_ids`: each row names 2 different experts of one group of 4 consecutive experts. In each aligned block of 256 rows (the rows of one device) no expert is named by more than 48 rows, and some expert is named by exactly 48 rows.
All inputs are finite; a program needn't handle non-finite values.
Results may differ from a plain program's by a relative error of at most 0.012.
Values may be sent and summed in bfloat16 or wider, within the bound.
A program may use at most 128 MiB of HBM per device.

v0:
```python
import jax
import jax.numpy as jnp
from jax import lax
from jax.sharding import PartitionSpec as P

GROUP_CH = 256
EXPERTS = 16
TOP = 2
CAP = 48
eps_norm = 1e-06


def from_behind(shard, axis, by):
    peers = lax.axis_size(axis)
    pairs = [(i, i + by) for i in range(peers) if 0 <= i + by < peers]
    return lax.ppermute(shard, axis, pairs)


def window_sums(extended, row_count):
    level_sum = extended
    stride = 1
    outputs = []
    for doubling in range(4):
        level_sum = level_sum[stride:] + level_sum[:-stride]
        stride = stride * 2
        outputs.append(level_sum[level_sum.shape[0] - row_count :])
    return outputs


def pool_mixer(pool_input, pool_gain):
    row_count, channels = pool_input.shape
    carried = from_behind(pool_input[row_count - 15 :], "ep", 1)
    extended = jnp.concatenate([carried, pool_input], axis=0).astype(jnp.float32)
    window_list = window_sums(extended, row_count)
    channel_ids = lax.axis_index("tp") * channels + lax.iota(jnp.int32, channels)
    group_ids = channel_ids // GROUP_CH
    position = lax.axis_index("ep") * row_count + lax.iota(jnp.int32, row_count)
    summed = jnp.zeros((row_count, channels), jnp.float32)
    widths = jnp.zeros((channels,), jnp.int32)
    for index_group in range(4):
        inside = group_ids == index_group
        summed = jnp.where(inside[None, :], window_list[index_group], summed)
        widths = jnp.where(inside, 2 ** (index_group + 1), widths)
    counted = jnp.minimum(position[:, None] + 1, widths[None, :]).astype(jnp.float32)
    values = extended[15:]
    return ((summed / counted - values) * pool_gain).astype(jnp.bfloat16)


def route_slots(expert_ids):
    flat_ids = expert_ids.reshape(-1)
    marked = (flat_ids[:, None] == lax.iota(jnp.int32, EXPERTS)[None, :]).astype(jnp.int32)
    before_count = jnp.cumsum(marked, axis=0) - marked
    ranked = jnp.sum(before_count * marked, axis=1)
    return (flat_ids * CAP + ranked).reshape(expert_ids.shape)


def body(
    pool_input,
    pool_gain,
    mix_weight,
    moe_input,
    moe_gain,
    expert_ids,
    route_weight,
    gate_weight,
    up_weight,
    down_weight,
):
    pooled = pool_mixer(pool_input, pool_gain)
    regrouped = lax.all_to_all(pooled, "tp", split_axis=0, concat_axis=1, tiled=True)
    mixed_sum = jnp.dot(
        regrouped,
        lax.all_gather(mix_weight, "tp", axis=0, tiled=True),
        preferred_element_type=jnp.float32,
    )
    mixed_out = mixed_sum.astype(jnp.bfloat16)
    inputs = moe_input.astype(jnp.float32)
    scale_rows = lax.rsqrt(jnp.mean(inputs * inputs, axis=-1, keepdims=True) + eps_norm)
    normed = (inputs * scale_rows * moe_gain).astype(jnp.bfloat16)
    slots = route_slots(expert_ids)
    slot_index = lax.iota(jnp.int32, EXPERTS * CAP)
    placing = (
        (slot_index[:, None] == slots[None, :, 0]) | (slot_index[:, None] == slots[None, :, 1])
    ).astype(jnp.bfloat16)
    outgoing = jnp.dot(placing, normed, preferred_element_type=jnp.float32).astype(jnp.bfloat16)
    outgoing = outgoing.reshape(EXPERTS, CAP, normed.shape[1])
    arrived = lax.all_to_all(outgoing, "ep", split_axis=0, concat_axis=1, tiled=True)
    gate_piece = lax.all_gather(gate_weight, "tp", axis=2, tiled=True)
    up_piece = lax.all_gather(up_weight, "tp", axis=2, tiled=True)
    down_piece = lax.all_gather(down_weight, "tp", axis=2, tiled=True)
    gate_part = jnp.einsum("erd,edf->erf", arrived, gate_piece, preferred_element_type=jnp.float32)
    upward = jnp.einsum("erd,edf->erf", arrived, up_piece, preferred_element_type=jnp.float32)
    hidden = (jax.nn.silu(gate_part) * upward).astype(jnp.bfloat16)
    expert_sum = jnp.einsum("erf,edf->erd", hidden, down_piece, preferred_element_type=jnp.float32)
    expert_rows = expert_sum.astype(jnp.bfloat16)
    returned = lax.all_to_all(expert_rows, "ep", split_axis=1, concat_axis=0, tiled=True)
    returned_rows = returned.reshape(EXPERTS * CAP, returned.shape[2])
    combined = jnp.zeros((normed.shape[0], normed.shape[1]), jnp.float32)
    for route_index in range(TOP):
        picking = (slots[:, route_index][:, None] == slot_index[None, :]).astype(jnp.bfloat16)
        chosen_rows = jnp.dot(picking, returned_rows, preferred_element_type=jnp.float32)
        combined = combined + route_weight[:, route_index : route_index + 1] * chosen_rows
    moe_out = combined.astype(jnp.bfloat16)
    return (mixed_out, moe_out)


def solution(mesh):
    return jax.shard_map(
        body,
        mesh=mesh,
        in_specs=(
            P("ep", "tp"),
            P("tp"),
            P("tp", None),
            P(("ep", "tp"), None),
            P(),
            P(("ep", "tp"), None),
            P(("ep", "tp"), None),
            P("ep", None, "tp"),
            P("ep", None, "tp"),
            P("ep", None, "tp"),
        ),
        out_specs=(P(("ep", "tp"), None), P(("ep", "tp"), None)),
        check_vma=False,
    )
```

profile of v0, /device:TPU:0, one launch (start us, length us, event | category | flops | bytes accessed | tf_op | source)
XLA Modules:
  0.0 554.3 jit_solution(15557223583954882724)
XLA Ops:
  9.9 1.2 reduce-window.6
  12.0 2.8 convolution_convert_fusion
  14.7 5.3 all-to-all-start.1
  20.1 3.9 collective-permute-start
  24.1 30.0 %collective-permute-done = bf16[15,128]{1,0:T(8,128)(2,1)S(1)} collective-permute-done((bf16[15,128]{1,0:T(8,128)(2,1)S(1)}, bf16[15,128]{1,0:T(8,128)(2,1)S(1)}, u32[]{:S(2)}, u32[]{:S(2)}) %collective-permute-start) | collective-permute-done | bytes 3872 | tf_op jit(solution)/shard_map/ppermute | solution.py:16
  54.4 1.1 fusion.12
  55.4 0.8 all-to-all-done.1
  56.2 5.2 all-to-all-start
  61.4 1.9 copy.51
  63.3 107.9 %all-gather.7.cloned.1.call-done = bf16[4,2048,1024]{2,1,0:T(8,128)(2,1)} async-done(((bf16[4,2048,128]{2,1,0:T(8,128)(2,1)}), bf16[4,2048,1024]{2,1,0:T(8,128)(2,1)}) %all-gather.7.cloned.1.call-update) | async-done | bytes 16777232 | tf_op jit(solution)/shard_map/all_gather | solution.py:88
  171.2 11.9 %fusion.28 = f32[4,192,1024]{2,1,0:T(8,128)} fusion(bf16[4,192,2048]{2,1,0:T(8,128)(2,1)} %bitcast.48, bf16[4,2048,1024]{2,1,0:T(8,128)(2,1)} %all-gather.7.cloned.1.call-done), kind=kOutput, calls=%fused_computation.62 | convolution fusion | flops 3221225472 | bytes 23068672 | tf_op jit(solution)/shard_map/erd,edf->erf/dot_general | solution.py:91
  183.2 142.6 %all-gather.11.cloned.1.call-done = bf16[4,2048,1024]{2,1,0:T(8,128)(2,1)} async-done(((bf16[4,2048,128]{2,1,0:T(8,128)(2,1)}), bf16[4,2048,1024]{2,1,0:T(8,128)(2,1)}) %all-gather.11.cloned.1.call-update) | async-done | bytes 16777232 | tf_op jit(solution)/shard_map/all_gather | solution.py:90
  325.8 151.6 %all-gather.9.cloned.1.call-done = bf16[4,2048,1024]{2,1,0:T(8,128)(2,1)} async-done(((bf16[4,2048,128]{2,1,0:T(8,128)(2,1)}), bf16[4,2048,1024]{2,1,0:T(8,128)(2,1)}) %all-gather.9.cloned.1.call-update) | async-done | bytes 16777232 | tf_op jit(solution)/shard_map/all_gather | solution.py:89
  477.4 17.7 %convolution_convert_fusion.1 = bf16[4,192,2048]{2,1,0:T(8,128)(2,1)} fusion(bf16[4,2048,1024]{2,1,0:T(8,128)(2,1)} %all-gather.11.cloned.1.call-done, f32[4,192,1024]{2,1,0:T(8,128)} %fusion.28, bf16[4,192,2048]{2,1,0:T(8,128)(2,1)S(1)} %bitcast.49, bf16[4,2048,1024]{2,1,0:T(8,128)(2,1)} %all-gather.9.cloned.1.call-done), kind=kOutput, calls=%fused_computation.1 | convolution fusion | flops 6448742400 | bytes 42991616 | tf_op jit(solution)/shard_map/erf,edf->erd/dot_general | solution.py:94
  495.1 6.0 %copy.52 = bf16[4,192,2048]{2,0,1:T(4,128)(2,1)} copy(bf16[4,192,2048]{2,1,0:T(8,128)(2,1)} %convolution_convert_fusion.1) | data formatting | bytes 6291456 | tf_op jit(solution)/shard_map/convert_element_type | solution.py:95
  501.1 0.7 copy-done.2
  501.8 3.9 all-to-all-start.2
  505.7 1.1 copy.46
  506.9 17.0 %all-gather.5.cloned.1.call-done = bf16[1024,2048]{1,0:T(8,128)(2,1)} async-done(((bf16[128,2048]{1,0:T(8,128)(2,1)}), bf16[1024,2048]{1,0:T(8,128)(2,1)}) %all-gather.5.cloned.1.call-update) | async-done | bytes 4194320 | tf_op jit(solution)/shard_map/all_gather | solution.py:73
  523.9 3.7 convolution_convert_fusion.2
  527.6 14.8 %all-to-all-done.2 = bf16[4,192,2048]{2,0,1:T(4,128)(2,1)S(1)} async-done(((bf16[4,192,2048]{2,0,1:T(4,128)(2,1)}), bf16[4,192,2048]{2,0,1:T(4,128)(2,1)S(1)}, u32[]{:S(2)}, u32[]{:S(2)}) %all-to-all-start.2) | async-done | bytes 3145760 | tf_op jit(solution)/shard_map/all_to_all | solution.py:96
  542.5 1.7 copy.53
  544.6 1.0 convolution_multiply_fusion.1
  545.7 2.1 fusion.1
  (49 shorter events, 4.2 us)
Async XLA Ops:
  7.2 2.3 copy-start.5
  7.2 4.4 copy-start.1
  7.2 164.1 %all-gather.7.cloned.1.call-start = ((), (), s32[]{:S(2)}) async-start(), calls=%async_computation.4 | async-start | bytes 18874368 | tf_op jit(solution)/shard_map/all_gather | solution.py:88
  7.9 4.0 copy-start.4
  7.9 317.8 %all-gather.11.cloned.1.call-start = ((), (), s32[]{:S(2)}) async-start(), calls=%async_computation.6 | async-start | bytes 18874368 | tf_op jit(solution)/shard_map/all_gather | solution.py:90
  8.7 468.7 %all-gather.9.cloned.1.call-start = ((), (), s32[]{:S(2)}) async-start(), calls=%async_computation.5 | async-start | bytes 18874368 | tf_op jit(solution)/shard_map/all_gather | solution.py:89
  14.7 5.3 copy-start.3
  14.7 41.5 %all-to-all-start.1 = ((bf16[16,48,2048]{2,1,0:T(8,128)(2,1)}), bf16[16,48,2048]{2,1,0:T(8,128)(2,1)S(1)}, u32[]{:S(2)}, u32[]{:S(2)}) async-start(bf16[16,48,2048]{2,1,0:T(8,128)(2,1)} %bitcast.7), calls=%async_computation.1 | async-start | bytes 6291456 | tf_op jit(solution)/shard_map/all_to_all | solution.py:87
  20.0 34.3 %copy-start.7 = (f32[128]{0:T(128)S(1)}, f32[128]{0:T(128)}, u32[]{:S(2)}) copy-start(f32[128]{0:T(128)} %param.11) | copy-start | bytes 1540
  20.0 503.9 %all-gather.5.cloned.1.call-start = ((), (), s32[]{:S(2)}) async-start(), calls=%async_computation.3 | async-start | bytes 4718592 | tf_op jit(solution)/shard_map/all_gather | solution.py:73
  20.1 34.0 %collective-permute-start = (bf16[15,128]{1,0:T(8,128)(2,1)S(1)}, bf16[15,128]{1,0:T(8,128)(2,1)S(1)}, u32[]{:S(2)}, u32[]{:S(2)}) collective-permute-start(bf16[15,128]{1,0:T(8,128)(2,1)S(1)} %slice.57), channel_id=1, source_target_pairs={{0,8},{8,16},{16,24},{1,9},{9,17},{17,25},{2,10},{10,18},{18,26},{... | collective-permute-start | bytes 11528 | tf_op jit(solution)/shard_map/ppermute | solution.py:16
  56.2 444.9 %all-to-all-start = ((bf16[8,128,128]{2,1,0:T(8,128)(2,1)}), bf16[8,128,128]{2,1,0:T(8,128)(2,1)S(1)}, u32[]{:S(2)}, u32[]{:S(2)}) async-start(bf16[8,128,128]{2,1,0:T(8,128)(2,1)} %bitcast), calls=%async_computation | async-start | bytes 524288 | tf_op jit(solution)/shard_map/all_to_all | solution.py:70
  171.2 306.1 %copy-start = (bf16[4,4,48,2048]{3,2,0,1:T(8,128)(2,1)S(1)}, bf16[4,4,48,2048]{3,2,0,1:T(8,128)(2,1)}, u32[]{:S(2)}) copy-start(bf16[4,4,48,2048]{3,2,0,1:T(8,128)(2,1)} %copy.51) | copy-start | bytes 9437188
  501.1 4.6 copy-start.6
  501.1 0.7 copy-start.2
  501.8 40.6 %all-to-all-start.2 = ((bf16[4,192,2048]{2,0,1:T(4,128)(2,1)}), bf16[4,192,2048]{2,0,1:T(4,128)(2,1)S(1)}, u32[]{:S(2)}, u32[]{:S(2)}) async-start(bf16[4,192,2048]{2,0,1:T(4,128)(2,1)} %copy.52), calls=%async_computation.2 | async-start | bytes 6291456 | tf_op jit(solution)/shard_map/all_to_all | solution.py:96
Sparse Core Ops, SparseCore 0:
  9.6 161.6 all-gather.6
  172.8 152.8 all-gather.10
  327.4 149.9 all-gather.8
  478.8 45.0 all-gather.4
where the time goes:
time: 555 us; the launch traced here: 554 us
  waiting for transfers between devices  467 us (84%)
  matrix products  39.2 us (7%)
  starting transfers between devices  18.4 us (3%)
  between operations  14 us (3%)
  local copies, waits for them, and re-layouts  12.8 us (2%)
    all_gather x1, waiting for transfers between devices, body(): up_piece = lax.all_gather(up_weight, 'tp', axis=2, tiled=True)  152 us
    all_gather x1, waiting for transfers between devices, body(): down_piece = lax.all_gather(down_weight, 'tp', axis=2, tiled=True)  143 us
    all_gather x1, waiting for transfers between devices, body(): gate_piece = lax.all_gather(gate_weight, 'tp', axis=2, tiled=True)  108 us
    ppermute x1, waiting for transfers between devices, from_behind(): return lax.ppermute(shard, axis, pairs)  30 us
    dot_general x1, matrix products, body(): jnp.einsum('erf,edf->erd', hidden, down_piece, preferred_element_type=jnp...  17.7 us
    all_gather x1, waiting for transfers between devices, body(): lax.all_gather(mix_weight, 'tp', axis=0, tiled=True)  17 us
    all_to_all x1, waiting for transfers between devices, body(): lax.all_to_all(expert_rows, 'ep', split_axis=1, concat_axis=0, tiled=True)  14.8 us
    dot_general x1, matrix products, body(): jnp.einsum('erd,edf->erf', arrived, gate_piece, preferred_element_type=jn...  11.9 us
  transfers between devices with their start and end apart: 8, of which 7 were waited for; matrix products, arithmetic and copies ran while one was open for 9% of the time, Pallas kernels for 0%

commit v1 on v0

--- a/solution.py
+++ b/solution.py
@@ -8,6 +8,22 @@
 TOP = 2
 CAP = 48
 eps_norm = 1e-06
+
+
+def ring_product(shard, axis, dim, term):
+    devices, mine, extent = (lax.axis_size(axis), lax.axis_index(axis), shard.shape[dim])
+    right = [(i, (i + 1) % devices) for i in range(devices)]
+    left = [(i, (i - 1) % devices) for i in range(devices)]
+    middle = devices // 2
+    from_left = from_right = shard
+    total = term(shard, mine * extent)
+    for step in range(1, middle + 1):
+        from_left = lax.ppermute(from_left, axis, right)
+        if step < devices - middle:
+            from_right = lax.ppermute(from_right, axis, left)
+            total = total + term(from_right, (mine + step) % devices * extent)
+        total = total + term(from_left, (mine - step) % devices * extent)
+    return total
 
 
 def from_behind(shard, axis, by):
@@ -87,11 +103,20 @@
     arrived = lax.all_to_all(outgoing, "ep", split_axis=0, concat_axis=1, tiled=True)
     gate_piece = lax.all_gather(gate_weight, "tp", axis=2, tiled=True)
     up_piece = lax.all_gather(up_weight, "tp", axis=2, tiled=True)
-    down_piece = lax.all_gather(down_weight, "tp", axis=2, tiled=True)
     gate_part = jnp.einsum("erd,edf->erf", arrived, gate_piece, preferred_element_type=jnp.float32)
     upward = jnp.einsum("erd,edf->erf", arrived, up_piece, preferred_element_type=jnp.float32)
     hidden = (jax.nn.silu(gate_part) * upward).astype(jnp.bfloat16)
-    expert_sum = jnp.einsum("erf,edf->erd", hidden, down_piece, preferred_element_type=jnp.float32)
+    expert_sum = ring_product(
+        down_weight,
+        "tp",
+        2,
+        lambda own_block, start: jnp.einsum(
+            "erf,edf->erd",
+            lax.dynamic_slice_in_dim(hidden, start, own_block.shape[2], axis=2),
+            own_block,
+            preferred_element_type=jnp.float32,
+        ),
+    )
     expert_rows = expert_sum.astype(jnp.bfloat16)
     returned = lax.all_to_all(expert_rows, "ep", split_axis=1, concat_axis=0, tiled=True)
     returned_rows = returned.reshape(EXPERTS * CAP, returned.shape[2])

time: 555 us -> 577 us (1.040)
  waiting for transfers between devices: 467 us -> 376 us
  starting transfers between devices: 18.4 us -> 81.8 us
  matrix products: 39.2 us -> 86 us
    ppermute x0 -> x7, waiting for transfers between devices: none -> 167 us  [the longest x4 167 us: ring_product(): from_left = lax.ppermute(from_left, axis, right)]
    all_gather x1 -> x0, waiting for transfers between devices: 143 us -> none  [body(): down_piece = lax.all_gather(down_weight, 'tp', axis=2, tiled=True)]
    all_gather x1, waiting for transfers between devices: 108 us -> 13.4 us  [body(): gate_piece = lax.all_gather(gate_weight, 'tp', axis=2, tiled=True)]
    dot_general x1 -> x9, matrix products: 17.7 us -> 64.4 us  [the longest x8 53.9 us: body(): jnp.einsum('erf,edf->erd', lax.dynamic_slice_in_dim(hidden, start, own_bl...]
    all_to_all x1, starting transfers between devices: 5.19 us -> 48 us  [body(): lax.all_to_all(pooled, 'tp', split_axis=0, concat_axis=1, tiled=True)]
    ppermute x1, waiting for transfers between devices: 30 us -> 0.01 us  [from_behind(): return lax.ppermute(shard, axis, pairs)]
    ppermute x0 -> x7, starting transfers between devices: none -> 20.5 us  [the longest x3 10.5 us: ring_product(): from_right = lax.ppermute(from_right, axis, left)]
    all_gather x1, waiting for transfers between devices: 17 us -> 0.02 us  [body(): lax.all_gather(mix_weight, 'tp', axis=0, tiled=True)]
  transfers between devices with their start and end apart: 8 -> 14, of which waited for: 7 -> 6; matrix products, arithmetic and copies ran while one was open for 9% -> 16% of each run, Pallas kernels for 0% -> 0%
where the time goes in v1:
time: 577 us; the launch traced here: 572 us
  waiting for transfers between devices  376 us (65%)
  matrix products  86 us (15%)
  starting transfers between devices  81.8 us (14%)
  between operations  14.1 us (2%)
  local copies, waits for them, and re-layouts  10.9 us (2%)
    ppermute x4, waiting for transfers between devices, ring_product(): from_left = lax.ppermute(from_left, axis, right)  167 us
    all_gather x1, waiting for transfers between devices, body(): up_piece = lax.all_gather(up_weight, 'tp', axis=2, tiled=True)  163 us
    dot_general x8, matrix products, body(): jnp.einsum('erf,edf->erd', lax.dynamic_slice_in_dim(hidden, start, own_bl...  53.9 us
    all_to_all x1, starting transfers between devices, body(): lax.all_to_all(pooled, 'tp', split_axis=0, concat_axis=1, tiled=True)  48 us
    all_to_all x1, waiting for transfers between devices, body(): lax.all_to_all(expert_rows, 'ep', split_axis=1, concat_axis=0, tiled=True)  31.6 us
    all_gather x1, waiting for transfers between devices, body(): gate_piece = lax.all_gather(gate_weight, 'tp', axis=2, tiled=True)  13.4 us
    dot_general x1, matrix products, body(): jnp.einsum('erd,edf->erf', arrived, gate_piece, preferred_element_type=jn...  12 us
  transfers between devices with their start and end apart: 14, of which 6 were waited for; matrix products, arithmetic and copies ran while one was open for 16% of the time, Pallas kernels for 0%

profile of v1, /device:TPU:0, one launch (start us, length us, event | category | flops | bytes accessed | tf_op | source)
XLA Modules:
  0.0 571.9 jit_solution(1898352420636539814)
XLA Ops:
  9.2 4.1 collective-permute-start.1
  13.3 74.5 %collective-permute-done.2 = bf16[4,2048,128]{2,1,0:T(8,128)(2,1)} collective-permute-done((bf16[4,2048,128]{2,1,0:T(8,128)(2,1)}, bf16[4,2048,128]{2,1,0:T(8,128)(2,1)}, u32[]{:S(2)}, u32[]{:S(2)}) %collective-permute-start.2) | collective-permute-done | bytes 2097184 | tf_op jit(solution)/shard_map/ppermute | solution.py:21
  93.9 5.2 all-to-all-start.1
  99.1 3.9 collective-permute-start
  106.0 63.2 %collective-permute-done.4 = bf16[4,2048,128]{2,1,0:T(8,128)(2,1)} collective-permute-done((bf16[4,2048,128]{2,1,0:T(8,128)(2,1)}, bf16[4,2048,128]{2,1,0:T(8,128)(2,1)}, u32[]{:S(2)}, u32[]{:S(2)}) %collective-permute-start.4) | collective-permute-done | bytes 2097184 | tf_op jit(solution)/shard_map/ppermute | solution.py:21
  169.2 8.7 %collective-permute-start.6 = (bf16[4,2048,128]{2,1,0:T(8,128)(2,1)}, bf16[4,2048,128]{2,1,0:T(8,128)(2,1)}, u32[]{:S(2)}, u32[]{:S(2)}) collective-permute-start(bf16[4,2048,128]{2,1,0:T(8,128)(2,1)} %collective-permute-done.4), channel_id=1, source_target_pairs={{0,1},{1,2},{2,3},{3,4},{4,5},{5,6},{6,7},{7,0},{8,9},{9,10},{10,1... | collective-permute-start | bytes 6291464 | tf_op jit(solution)/shard_map/ppermute | solution.py:21
  179.4 48.0 %all-to-all-start = ((bf16[8,128,128]{2,1,0:T(8,128)(2,1)}), bf16[8,128,128]{2,1,0:T(8,128)(2,1)S(1)}, u32[]{:S(2)}, u32[]{:S(2)}) async-start(bf16[8,128,128]{2,1,0:T(8,128)(2,1)} %bitcast), calls=%async_computation | async-start | bytes 524288 | tf_op jit(solution)/shard_map/all_to_all | solution.py:86
  232.8 28.9 %collective-permute-done.6 = bf16[4,2048,128]{2,1,0:T(8,128)(2,1)} collective-permute-done((bf16[4,2048,128]{2,1,0:T(8,128)(2,1)}, bf16[4,2048,128]{2,1,0:T(8,128)(2,1)}, u32[]{:S(2)}, u32[]{:S(2)}) %collective-permute-start.6) | collective-permute-done | bytes 2097184 | tf_op jit(solution)/shard_map/ppermute | solution.py:21
  261.7 13.4 %all-gather.6.cloned.1.call-done = bf16[4,2048,1024]{2,1,0:T(8,128)(2,1)} async-done(((bf16[4,2048,128]{2,1,0:T(8,128)(2,1)}), bf16[4,2048,1024]{2,1,0:T(8,128)(2,1)}) %all-gather.6.cloned.1.call-update) | async-done | bytes 16777232 | tf_op jit(solution)/shard_map/all_gather | solution.py:104
  275.1 12.0 %fusion.49 = f32[4,192,1024]{2,1,0:T(8,128)} fusion(bf16[4,192,2048]{2,1,0:T(8,128)(2,1)} %bitcast.55, bf16[4,2048,1024]{2,1,0:T(8,128)(2,1)} %all-gather.6.cloned.1.call-done), kind=kOutput, calls=%fused_computation.83 | convolution fusion | flops 3221225472 | bytes 23068672 | tf_op jit(solution)/shard_map/erd,edf->erf/dot_general | solution.py:106
  287.1 163.1 %all-gather.8.cloned.1.call-done = bf16[4,2048,1024]{2,1,0:T(8,128)(2,1)} async-done(((bf16[4,2048,128]{2,1,0:T(8,128)(2,1)}), bf16[4,2048,1024]{2,1,0:T(8,128)(2,1)}) %all-gather.8.cloned.1.call-update) | async-done | bytes 16777232 | tf_op jit(solution)/shard_map/all_gather | solution.py:105
  450.3 10.4 %multiply_convert_fusion = bf16[4,192,1024]{2,1,0:T(8,128)(2,1)S(1)} fusion(f32[4,192,1024]{2,1,0:T(8,128)} %fusion.49, bf16[4,192,2048]{2,1,0:T(8,128)(2,1)S(1)} %bitcast.56, bf16[4,2048,1024]{2,1,0:T(8,128)(2,1)} %all-gather.8.cloned.1.call-done), kind=kOutput, calls=%fused_computation.2 | convolution fusion | flops 3225944064 | bytes 24641536 | tf_op jit(solution)/shard_map/erd,edf->erf/dot_general | solution.py:107
  460.7 5.9 %fusion.33 = f32[4,192,2048]{2,1,0:T(8,128)} fusion(bf16[4,2048,128]{2,1,0:T(8,128)(2,1)} %param.19, bf16[4,192,1024]{2,1,0:T(8,128)(2,1)S(1)} %multiply_convert_fusion, s32[]{:T(128)S(6)} %select_n.127), kind=kOutput, calls=%fused_computation.50 | convolution fusion | flops 402653184 | bytes 8585220 | tf_op jit(solution)/shard_map/erf,edf->erd/dot_general | solution.py:113
  466.6 5.2 fusion.25
  471.8 5.2 fusion.27
  477.1 5.2 fusion.29
  482.3 5.3 fusion.31
  487.5 5.2 fusion.21
  492.7 5.2 fusion.23
  497.9 16.8 %add_convert_fusion = bf16[4,192,2048]{2,1,0:T(8,128)(2,1)S(1)} fusion(f32[4,192,2048]{2,1,0:T(8,128)} %fusion.21, f32[4,192,2048]{2,1,0:T(8,128)} %fusion.23, f32[4,192,2048]{2,1,0:T(8,128)} %fusion.25, f32[4,192,2048]{2,1,0:T(8,128)} %fusion.27, f32[4,192,2048]{2,1,0:T(8,128)} %fusion.29, f32[4,192,2048]{2,1,0:T(8,128)} %fusion.33, ...), kind=kOutput, calls=%fused_computation | convolution fusion | flops 415236096 | bytes 49479684 | tf_op jit(solution)/shard_map/erf,edf->erd/dot_general | solution.py:113
  514.7 4.1 copy.52
  519.5 4.1 all-to-all-start.2
  524.8 3.7 convolution_convert_fusion.1
  528.5 31.6 %all-to-all-done.2 = bf16[4,192,2048]{2,0,1:T(4,128)(2,1)S(1)} async-done(((bf16[4,192,2048]{2,0,1:T(4,128)(2,1)}), bf16[4,192,2048]{2,0,1:T(4,128)(2,1)S(1)}, u32[]{:S(2)}, u32[]{:S(2)}) %all-to-all-start.2) | async-done | bytes 3145760 | tf_op jit(solution)/shard_map/all_to_all | solution.py:121
  (70 shorter events, 24.8 us)
Async XLA Ops:
  7.2 81.4 %copy-start.6 = (s32[256,2]{0,1:T(2,128)S(1)}, s32[256,2]{0,1:T(2,128)}, u32[]{:S(2)}) copy-start(s32[256,2]{0,1:T(2,128)} %param.15) | copy-start | bytes 6148
  7.2 83.6 %copy-start.1 = (bf16[256,2048]{1,0:T(8,128)(2,1)S(1)}, bf16[256,2048]{1,0:T(8,128)(2,1)}, u32[]{:S(2)}) copy-start(bf16[256,2048]{1,0:T(8,128)(2,1)} %param.13) | copy-start | bytes 3145732
  7.2 83.9 %copy-start.5 = (f32[2048]{0:T(1024)S(1)}, f32[2048]{0:T(1024)}, u32[]{:S(2)}) copy-start(f32[2048]{0:T(1024)} %param.14) | copy-start | bytes 24580
  7.2 268.0 %all-gather.6.cloned.1.call-start = ((), (), s32[]{:S(2)}) async-start(), calls=%async_computation.4 | async-start | bytes 18874368 | tf_op jit(solution)/shard_map/all_gather | solution.py:104
  7.9 442.3 %all-gather.8.cloned.1.call-start = ((), (), s32[]{:S(2)}) async-start(), calls=%async_computation.5 | async-start | bytes 18874368 | tf_op jit(solution)/shard_map/all_gather | solution.py:105
  8.7 79.2 %collective-permute-start.2 = (bf16[4,2048,128]{2,1,0:T(8,128)(2,1)}, bf16[4,2048,128]{2,1,0:T(8,128)(2,1)}, u32[]{:S(2)}, u32[]{:S(2)}) collective-permute-start(bf16[4,2048,128]{2,1,0:T(8,128)(2,1)} %param.19), channel_id=1, source_target_pairs={{0,1},{1,2},{2,3},{3,4},{4,5},{5,6},{6,7},{7,0},{8,9},{9,10},{10,1... | collective-permute-start | bytes 6291464 | tf_op jit(solution)/shard_map/ppermute | solution.py:21
  9.2 93.9 %collective-permute-start.1 = (bf16[4,2048,128]{2,1,0:T(8,128)(2,1)}, bf16[4,2048,128]{2,1,0:T(8,128)(2,1)}, u32[]{:S(2)}, u32[]{:S(2)}) collective-permute-start(bf16[4,2048,128]{2,1,0:T(8,128)(2,1)} %param.19), channel_id=1, source_target_pairs={{0,7},{1,0},{2,1},{3,2},{4,3},{5,4},{6,5},{7,6},{8,15},{9,8},{10,9... | collective-permute-start | bytes 6291464 | tf_op jit(solution)/shard_map/ppermute | solution.py:23
  87.9 81.3 %collective-permute-start.4 = (bf16[4,2048,128]{2,1,0:T(8,128)(2,1)}, bf16[4,2048,128]{2,1,0:T(8,128)(2,1)}, u32[]{:S(2)}, u32[]{:S(2)}) collective-permute-start(bf16[4,2048,128]{2,1,0:T(8,128)(2,1)} %collective-permute-done.2), channel_id=1, source_target_pairs={{0,1},{1,2},{2,3},{3,4},{4,5},{5,6},{6,7},{7,0},{8,9},{9,10},{10,1... | collective-permute-start | bytes 6291464 | tf_op jit(solution)/shard_map/ppermute | solution.py:21
  93.9 5.2 copy-start.4
  93.9 85.5 %all-to-all-start.1 = ((bf16[16,48,2048]{2,1,0:T(8,128)(2,1)}), bf16[16,48,2048]{2,1,0:T(8,128)(2,1)S(1)}, u32[]{:S(2)}, u32[]{:S(2)}) async-start(bf16[16,48,2048]{2,1,0:T(8,128)(2,1)} %bitcast.7), calls=%async_computation.1 | async-start | bytes 6291456 | tf_op jit(solution)/shard_map/all_to_all | solution.py:103
  99.1 425.8 %all-gather.4.cloned.1.call-start = ((), (), s32[]{:S(2)}) async-start(), calls=%async_computation.3 | async-start | bytes 4718592 | tf_op jit(solution)/shard_map/all_gather | solution.py:89
  99.1 79.2 %copy-start.8 = (f32[128]{0:T(128)S(1)}, f32[128]{0:T(128)}, u32[]{:S(2)}) copy-start(f32[128]{0:T(128)} %param.11) | copy-start | bytes 1540
  99.1 79.0 %collective-permute-start = (bf16[15,128]{1,0:T(8,128)(2,1)S(1)}, bf16[15,128]{1,0:T(8,128)(2,1)S(1)}, u32[]{:S(2)}, u32[]{:S(2)}) collective-permute-start(bf16[15,128]{1,0:T(8,128)(2,1)S(1)} %slice.57), channel_id=1, source_target_pairs={{0,8},{8,16},{16,24},{1,9},{9,17},{17,25},{2,10},{10,18},{18,26},{... | collective-permute-start | bytes 11528 | tf_op jit(solution)/shard_map/ppermute | solution.py:32
  103.1 126.2 %collective-permute-start.3 = (bf16[4,2048,128]{2,1,0:T(8,128)(2,1)}, bf16[4,2048,128]{2,1,0:T(8,128)(2,1)}, u32[]{:S(2)}, u32[]{:S(2)}) collective-permute-start(bf16[4,2048,128]{2,1,0:T(8,128)(2,1)} %collective-permute-done.1), channel_id=1, source_target_pairs={{0,7},{1,0},{2,1},{3,2},{4,3},{5,4},{6,5},{7,6},{8,15},{9,8},{10,9... | collective-permute-start | bytes 6291464 | tf_op jit(solution)/shard_map/ppermute | solution.py:23
  169.2 92.5 %collective-permute-start.6 = (bf16[4,2048,128]{2,1,0:T(8,128)(2,1)}, bf16[4,2048,128]{2,1,0:T(8,128)(2,1)}, u32[]{:S(2)}, u32[]{:S(2)}) collective-permute-start(bf16[4,2048,128]{2,1,0:T(8,128)(2,1)} %collective-permute-done.4), channel_id=1, source_target_pairs={{0,1},{1,2},{2,3},{3,4},{4,5},{5,6},{6,7},{7,0},{8,9},{9,10},{10,1... | collective-permute-start | bytes 6291464 | tf_op jit(solution)/shard_map/ppermute | solution.py:21
  179.4 339.4 %all-to-all-start = ((bf16[8,128,128]{2,1,0:T(8,128)(2,1)}), bf16[8,128,128]{2,1,0:T(8,128)(2,1)S(1)}, u32[]{:S(2)}, u32[]{:S(2)}) async-start(bf16[8,128,128]{2,1,0:T(8,128)(2,1)} %bitcast), calls=%async_computation | async-start | bytes 524288 | tf_op jit(solution)/shard_map/all_to_all | solution.py:86
  229.3 263.4 %collective-permute-start.5 = (bf16[4,2048,128]{2,1,0:T(8,128)(2,1)}, bf16[4,2048,128]{2,1,0:T(8,128)(2,1)}, u32[]{:S(2)}, u32[]{:S(2)}) collective-permute-start(bf16[4,2048,128]{2,1,0:T(8,128)(2,1)} %collective-permute-done.3), channel_id=1, source_target_pairs={{0,7},{1,0},{2,1},{3,2},{4,3},{5,4},{6,5},{7,6},{8,15},{9,8},{10,9... | collective-permute-start | bytes 6291464 | tf_op jit(solution)/shard_map/ppermute | solution.py:23
  261.7 236.2 %collective-permute-start.7 = (bf16[4,2048,128]{2,1,0:T(8,128)(2,1)}, bf16[4,2048,128]{2,1,0:T(8,128)(2,1)}, u32[]{:S(2)}, u32[]{:S(2)}) collective-permute-start(bf16[4,2048,128]{2,1,0:T(8,128)(2,1)} %collective-permute-done.6), channel_id=1, source_target_pairs={{0,1},{1,2},{2,3},{3,4},{4,5},{5,6},{6,7},{7,0},{8,9},{9,10},{10,1... | collective-permute-start | bytes 6291464 | tf_op jit(solution)/shard_map/ppermute | solution.py:21
  275.1 175.1 %copy-start = (bf16[4,4,48,2048]{3,2,0,1:T(8,128)(2,1)S(1)}, bf16[4,4,48,2048]{3,2,0,1:T(8,128)(2,1)}, u32[]{:S(2)}) copy-start(bf16[4,4,48,2048]{3,2,0,1:T(8,128)(2,1)} %copy.51) | copy-start | bytes 9437188
  460.7 32.0 %copy-start.2 = (bf16[4,192,1024]{2,1,0:T(8,128)(2,1)}, bf16[4,192,1024]{2,1,0:T(8,128)(2,1)S(1)}, u32[]{:S(2)}) copy-start(bf16[4,192,1024]{2,1,0:T(8,128)(2,1)S(1)} %multiply_convert_fusion) | copy-start | bytes 4718596
  518.8 4.9 copy-start.7
  518.8 0.7 copy-start.3
  519.5 40.6 %all-to-all-start.2 = ((bf16[4,192,2048]{2,0,1:T(4,128)(2,1)}), bf16[4,192,2048]{2,0,1:T(4,128)(2,1)S(1)}, u32[]{:S(2)}, u32[]{:S(2)}) async-start(bf16[4,192,2048]{2,0,1:T(4,128)(2,1)} %copy.52), calls=%async_computation.2 | async-start | bytes 6291456 | tf_op jit(solution)/shard_map/all_to_all | solution.py:121
Sparse Core Ops, SparseCore 0:
  9.6 265.5 all-gather.5
  276.7 173.4 all-gather.7
  451.9 53.2 all-gather.3
